TPU v7x, 32 devices: a whole 2x2x4 slice. The times are simulated.
32 devices in a mesh: grp: 2 (over y), sp: 4 (over z), tp: 4 (over x, core).
Axes of the slice: x: 2, y: 2, z: 4, core: 2. Of those that a mesh axis runs over, the one named last changes fastest.
Arguments:
- queries: bfloat16 [4096, 1024], P(('grp', 'sp'), 'tp'), parts along dimension 0, may hold values from -120 to 120
- keys: bfloat16 [4096, 256], P(('grp', 'sp')), parts along dimension 0, may hold values from -6 to 6
- values: bfloat16 [4096, 256], P(('grp', 'sp')), parts along dimension 0, may hold values from -6 to 6
- sink: float32 [8], P('tp'), may hold values from 1 to 5
- resid: bfloat16 [4096, 2048], P(('grp', 'sp')), parts along dimension 0, may hold values from -100 to 100
- out_proj: bfloat16 [1024, 2048], P(None, 'tp'), may hold values from -1.5 to 1.5
- norm_gain: float32 [2048], replicated, may hold values from 0.1 to 1.9
- w_gate: bfloat16 [2048, 6144], P('sp', 'tp'), may hold values from -0.125 to 0.125
- w_up: bfloat16 [2048, 6144], P('sp', 'tp'), may hold values from -0.125 to 0.125
- conv_w: float32 [3, 6144], P(None, 'tp'), may hold values from -3 to 3
- conv_b: float32 [6144], P('tp'), may hold values from -3 to 3
- w_down: bfloat16 [6144, 2048], P('tp', 'sp'), may hold values from -0.21875 to 0.21875
Outputs:
- layer_out: bfloat16 [4096, 2048], P(('grp', 'sp'), 'tp'), parts along dimension 0
There are 2 independent parts, one for each index of `grp`. A program takes and returns all parts, laid end to end along the dimension named above; an argument that names none is the same for every part. Nothing has to cross between parts.
All inputs are finite; a program needn't handle non-finite values.
Results may differ from a plain program's by a relative error of at most 0.015.
Values may be sent and summed in bfloat16 or wider, within the bound.
A program may use at most 64 MiB of HBM per device.

v0:
```python
import jax
import jax.numpy as jnp
from jax import lax
from jax.sharding import PartitionSpec as P

H = 8
KVH = 2
HD = 128
WINDOW = 128
CONV = 3


def with_halo(cells, sides, width):
    for axis, dim in sides:
        count = lax.axis_size(axis)
        ends = count - 1
        head = lax.slice_in_dim(cells, 0, width, axis=dim)
        tail = lax.slice_in_dim(cells, cells.shape[dim] - width, cells.shape[dim], axis=dim)
        cells = jnp.concatenate(
            [
                lax.ppermute(tail, axis, [(i, (i + 1) % count) for i in range(ends)]),
                cells,
                lax.ppermute(head, axis, [((i + 1) % count, i) for i in range(ends)]),
            ],
            axis=dim,
        )
    return cells


def shards(
    queries, keys, values, sink, resid, out_proj, norm_gain, w_gate, w_up, conv_w, conv_b, w_down
):
    tokens = queries.shape[0]
    width = resid.shape[1]
    heads_here = sink.shape[0]
    group = H // KVH
    scale = HD ** (-0.5)
    first_head = lax.axis_index("tp") * heads_here
    kv_head = first_head // group
    own_keys = lax.dynamic_slice_in_dim(keys, kv_head * HD, HD, 1)
    own_values = lax.dynamic_slice_in_dim(values, kv_head * HD, HD, 1)
    extended = with_halo(jnp.stack([own_keys, own_values]), (("sp", 1),), WINDOW)
    ext_keys = extended[0]
    ext_values = extended[1]
    span = tokens + 2 * WINDOW
    q_heads = queries.reshape(tokens, heads_here, HD)
    scores = (
        jnp.einsum("qhd,kd->hqk", q_heads, ext_keys, preferred_element_type=jnp.float32) * scale
    )
    offset = lax.axis_index("sp") * tokens
    q_pos = offset + jnp.arange(tokens, dtype=jnp.int32)[:, None]
    k_pos = offset - WINDOW + jnp.arange(span, dtype=jnp.int32)[None, :]
    seq_total = tokens * lax.axis_size("sp")
    valid = (jnp.abs(q_pos - k_pos) <= WINDOW) & (k_pos >= 0) & (k_pos < seq_total)
    scores = jnp.where(valid[None], scores, jnp.float32(-1e30))
    sink_col = sink[:, None]
    top = jnp.maximum(jnp.max(scores, axis=-1), sink_col)
    expo = jnp.exp(scores - top[..., None])
    total = jnp.sum(expo, axis=-1) + jnp.exp(sink_col - top)
    weights = (expo / total[..., None]).astype(jnp.bfloat16)
    heads_out = jnp.einsum("hqk,kd->qhd", weights, ext_values, preferred_element_type=jnp.float32)
    heads_out = heads_out.astype(jnp.bfloat16).reshape(tokens, heads_here * HD)
    all_heads = lax.all_gather(heads_out, "tp", axis=1, tiled=True)
    cols = width // lax.axis_size("tp")
    col_start = lax.axis_index("tp") * cols
    full_proj = lax.all_gather(out_proj, "tp", axis=1, tiled=True)
    summed = resid.astype(jnp.float32) + jnp.dot(
        all_heads, full_proj, preferred_element_type=jnp.float32
    )
    mean = jnp.mean(summed, axis=-1, keepdims=True)
    msq = jnp.mean(summed * summed, axis=-1, keepdims=True)
    normed_full = ((summed - mean) * lax.rsqrt(msq - mean * mean + 1e-05) * norm_gain).astype(
        jnp.bfloat16
    )
    normed_own = lax.dynamic_slice_in_dim(normed_full, col_start, cols, 1)
    gate_acc = jnp.dot(
        normed_full,
        lax.all_gather(w_gate, "sp", axis=0, tiled=True),
        preferred_element_type=jnp.float32,
    )
    up_acc = jnp.dot(
        normed_full,
        lax.all_gather(w_up, "sp", axis=0, tiled=True),
        preferred_element_type=jnp.float32,
    )
    gate_pre = gate_acc.astype(jnp.bfloat16)
    up_part = up_acc.astype(jnp.bfloat16)
    padded = with_halo(gate_pre, (("sp", 0),), CONV // 2)
    conv = conv_b
    for tap in range(CONV):
        conv = conv + padded[tap : tap + tokens].astype(jnp.float32) * conv_w[tap]
    act = (jax.nn.silu(conv) * up_part.astype(jnp.float32)).astype(jnp.bfloat16)
    terms = jnp.dot(
        act, lax.all_gather(w_down, "sp", axis=1, tiled=True), preferred_element_type=jnp.float32
    )
    ffn_own = lax.psum_scatter(
        terms.astype(jnp.bfloat16), "tp", scatter_dimension=1, tiled=True
    ).astype(jnp.float32)
    return (normed_own.astype(jnp.float32) + ffn_own).astype(jnp.bfloat16)


def solution(mesh):
    return jax.shard_map(
        shards,
        mesh=mesh,
        in_specs=(
            P(("grp", "sp"), "tp"),
            P(("grp", "sp"), None),
            P(("grp", "sp"), None),
            P("tp"),
            P(("grp", "sp"), None),
            P(None, "tp"),
            P(),
            P("sp", "tp"),
            P("sp", "tp"),
            P(None, "tp"),
            P("tp"),
            P("tp", "sp"),
        ),
        out_specs=P(("grp", "sp"), "tp"),
        check_vma=False,
    )
```

profile of v0, /device:TPU:0, one launch (start us, length us, event | category | flops | bytes accessed | tf_op | source)
XLA Modules:
  0.0 476.0 jit_solution(9016852230966235995)
XLA Ops:
  6.5 1.0 dynamic-slice_bitcast_fusion
  7.6 5.0 %collective-permute-start = (bf16[2,128,128]{2,1,0:T(8,128)(2,1)S(1)}, bf16[2,128,128]{2,1,0:T(8,128)(2,1)S(1)}, u32[]{:S(2)}, u32[]{:S(2)}) collective-permute-start(bf16[2,128,128]{2,1,0:T(8,128)(2,1)S(1)} %get-tuple-element.12), channel_id=1, source_target_pairs={{0,4},{4,8},{8,12},{1,5},{5,9},{9,13},{2,6},{6,10},{10,14},{3,7},{... | collective-permute-start | bytes 196616 | tf_op jit(solution)/shard_map/ppermute | solution.py:21
  12.6 1.3 collective-permute-start.1
  13.9 0.8 fusion.10
  14.7 4.0 collective-permute-done.1
  18.8 0.8 fusion.1
  19.5 0.1 broadcast_maximum_fusion
  19.6 0.7 fusion
  20.3 0.1 exponential_add_fusion
  20.4 1.9 fusion.12
  22.3 0.0 all-gather.8.cloned.1.call-start
  22.3 0.7 all-gather.8.cloned.1.call-update
  23.1 0.7 all-gather.10.cloned.1.call-update
  23.8 0.0 all-gather.12.cloned.1.call-start
  23.8 0.5 all-gather.12.cloned.1.call-update
  24.4 0.0 all-gather.14.cloned.1.call-start
  24.4 0.5 all-gather.14.cloned.1.call-update
  25.0 0.0 reduce-scatter.2.cloned.1.call-start
  25.0 14.4 %all-gather.6.cloned.1.call-done = bf16[512,1024]{0,1:T(8,128)(2,1)} async-done(((bf16[512,256]{0,1:T(8,128)(2,1)}), bf16[512,1024]{0,1:T(8,128)(2,1)}) %all-gather.6.cloned.1.call-update) | async-done | bytes 1048592 | tf_op jit(solution)/shard_map/all_gather | solution.py:63
  39.4 36.0 %all-gather.8.cloned.1.call-done = bf16[1024,2048]{1,0:T(8,128)(2,1)} async-done(((bf16[1024,512]{1,0:T(8,128)(2,1)}), bf16[1024,2048]{1,0:T(8,128)(2,1)}) %all-gather.8.cloned.1.call-update) | async-done | bytes 4194320 | tf_op jit(solution)/shard_map/all_gather | solution.py:66
  75.4 5.4 %fusion.22 = (f32[512]{0:T(512)S(1)}, f32[512]{0:T(512)S(1)}, f32[512,2048]{1,0:T(8,128)S(1)}) fusion(bf16[512,1024]{0,1:T(8,128)(2,1)} %all-gather.6.cloned.1.call-done, bf16[1024,2048]{1,0:T(8,128)(2,1)} %all-gather.8.cloned.1.call-done, bf16[512,2048]{1,0:T(8,128)(2,1)S(1)} %copy-done.5), kind=kOutput, calls=%fused_computation.52 | convolution fusion | flops 2152725504 | bytes 11538432 | tf_op jit(solution)/shard_map/dot_general | solution.py:67
  80.8 0.6 multiply_convert_fusion
  81.5 110.9 %all-gather.10.cloned.1.call-done = bf16[2048,1536]{1,0:T(8,128)(2,1)} async-done(((bf16[512,1536]{1,0:T(8,128)(2,1)}), bf16[2048,1536]{1,0:T(8,128)(2,1)}) %all-gather.10.cloned.1.call-update) | async-done | bytes 6291472 | tf_op jit(solution)/shard_map/all_gather | solution.py:78
  192.4 6.2 %convolution_convert_fusion.2 = bf16[512,1536]{1,0:T(8,128)(2,1)S(1)} fusion(bf16[512,2048]{1,0:T(8,128)(2,1)S(1)} %multiply_convert_fusion, bf16[2048,1536]{1,0:T(8,128)(2,1)} %all-gather.10.cloned.1.call-done), kind=kOutput, calls=%fused_computation.9 | convolution fusion | flops 3222011904 | bytes 9961472 | tf_op jit(solution)/shard_map/dot_general | solution.py:76
  198.6 1.3 collective-permute-start.2
  199.9 1.5 collective-permute-start.3
  201.4 0.1 slice_reduce_fusion.2
  201.5 105.9 %all-gather.12.cloned.1.call-done = bf16[2048,1536]{1,0:T(8,128)(2,1)} async-done(((bf16[512,1536]{1,0:T(8,128)(2,1)}), bf16[2048,1536]{1,0:T(8,128)(2,1)}) %all-gather.12.cloned.1.call-update) | async-done | bytes 6291472 | tf_op jit(solution)/shard_map/all_gather | solution.py:83
  307.4 114.9 %all-gather.14.cloned.1.call-done = bf16[1536,2048]{1,0:T(8,128)(2,1)} async-done(((bf16[1536,512]{1,0:T(8,128)(2,1)}), bf16[1536,2048]{1,0:T(8,128)(2,1)}) %all-gather.14.cloned.1.call-update) | async-done | bytes 6291472 | tf_op jit(solution)/shard_map/all_gather | solution.py:94
  422.3 15.3 %convolution_convert_fusion = bf16[512,2048]{1,0:T(8,128)(2,1)} fusion(bf16[1536,2048]{1,0:T(8,128)(2,1)} %all-gather.14.cloned.1.call-done, bf16[512,1536]{1,0:T(8,128)(2,1)} %copy-done.4, bf16[1,1536]{1,0:T(2,128)(2,1)S(1)} %collective-permute-done.3, bf16[1,1536]{1,0:T(2,128)(2,1)S(1)} %collective-permute-done.2, f32[1536]{0:T(1024)S(1)} %get-tuple-element.8, ...), kind=kOutput, calls=%fused_computation.7 | convolution fusion | flops 6461587456 | bytes 18380800 | tf_op jit(solution)/shard_map/dot_general | solution.py:93
  437.6 29.5 %reduce-scatter.2.cloned.1.call-done = bf16[512,512]{1,0:T(8,128)(2,1)} async-done(((bf16[512,2048]{1,0:T(8,128)(2,1)}), bf16[512,512]{1,0:T(8,128)(2,1)}) %reduce-scatter.2.cloned.1.call-update) | async-done | bytes 524304 | tf_op jit(solution)/shard_map/reduce_scatter | solution.py:96
  467.1 2.0 add_convert_fusion
  (28 shorter events, 0.2 us)
Async XLA Ops:
  6.5 12.2 %copy-start = (bf16[512,256]{1,0:T(8,128)(2,1)S(1)}, bf16[512,256]{1,0:T(8,128)(2,1)}, u32[]{:S(2)}) copy-start(bf16[512,256]{1,0:T(8,128)(2,1)} %param.12) | copy-start | bytes 786436
  6.5 32.8 %all-gather.6.cloned.1.call-start = ((), (), s32[]{:S(2)}) async-start(), calls=%async_computation.1 | async-start | bytes 1310720 | tf_op jit(solution)/shard_map/all_gather | solution.py:63
  6.5 13.0 %copy-start.3 = (f32[2]{0:T(128)S(1)}, f32[2]{0:T(128)}, u32[]{:S(2)}) copy-start(f32[2]{0:T(128)} %param.15) | copy-start | bytes 28
  7.6 7.1 %collective-permute-start = (bf16[2,128,128]{2,1,0:T(8,128)(2,1)S(1)}, bf16[2,128,128]{2,1,0:T(8,128)(2,1)S(1)}, u32[]{:S(2)}, u32[]{:S(2)}) collective-permute-start(bf16[2,128,128]{2,1,0:T(8,128)(2,1)S(1)} %get-tuple-element.12), channel_id=1, source_target_pairs={{0,4},{4,8},{8,12},{1,5},{5,9},{9,13},{2,6},{6,10},{10,14},{3,7},{... | collective-permute-start | bytes 196616 | tf_op jit(solution)/shard_map/ppermute | solution.py:21
  12.6 6.2 %collective-permute-start.1 = (bf16[2,128,128]{2,1,0:T(8,128)(2,1)S(1)}, bf16[2,128,128]{2,1,0:T(8,128)(2,1)S(1)}, u32[]{:S(2)}, u32[]{:S(2)}) collective-permute-start(bf16[2,128,128]{2,1,0:T(8,128)(2,1)S(1)} %get-tuple-element.13), channel_id=1, source_target_pairs={{4,0},{8,4},{12,8},{5,1},{9,5},{13,9},{6,2},{10,6},{14,10},{7,3},{... | collective-permute-start | bytes 196616 | tf_op jit(solution)/shard_map/ppermute | solution.py:23
  22.3 53.2 %copy-start.5 = (bf16[512,2048]{1,0:T(8,128)(2,1)S(1)}, bf16[512,2048]{1,0:T(8,128)(2,1)}, u32[]{:S(2)}) copy-start(bf16[512,2048]{1,0:T(8,128)(2,1)} %param.16) | copy-start | bytes 6291460
  22.3 53.1 %all-gather.8.cloned.1.call-start = ((), (), s32[]{:S(2)}) async-start(), calls=%async_computation.2 | async-start | bytes 5242880 | tf_op jit(solution)/shard_map/all_gather | solution.py:66
  23.1 169.3 %all-gather.10.cloned.1.call-start = ((), (), s32[]{:S(2)}) async-start(), calls=%async_computation.3 | async-start | bytes 7864320 | tf_op jit(solution)/shard_map/all_gather | solution.py:78
  23.8 283.6 %all-gather.12.cloned.1.call-start = ((), (), s32[]{:S(2)}) async-start(), calls=%async_computation.4 | async-start | bytes 7864320 | tf_op jit(solution)/shard_map/all_gather | solution.py:83
  24.4 398.0 %all-gather.14.cloned.1.call-start = ((), (), s32[]{:S(2)}) async-start(), calls=%async_computation.5 | async-start | bytes 7864320 | tf_op jit(solution)/shard_map/all_gather | solution.py:94
  24.9 55.9 %copy-start.2 = (f32[2048]{0:T(1024)S(1)}, f32[2048]{0:T(1024)}, u32[]{:S(2)}) copy-start(f32[2048]{0:T(1024)} %param.18) | copy-start | bytes 24580
  25.0 442.2 %reduce-scatter.2.cloned.1.call-start = ((), (), s32[]{:S(2)}) async-start(), calls=%async_computation.6 | async-start | bytes 2621440 | tf_op jit(solution)/shard_map/reduce_scatter | solution.py:96
  81.5 119.9 %copy-start.1 = (f32[3,1536]{1,0:T(4,128)S(1)}, f32[3,1536]{1,0:T(4,128)}, u32[]{:S(2)}) copy-start(f32[3,1536]{1,0:T(4,128)} %param.21) | copy-start | bytes 55300
  81.5 340.9 %copy-start.6 = (f32[1536]{0:T(1024)S(1)}, f32[1536]{0:T(1024)}, u32[]{:S(2)}) copy-start(f32[1536]{0:T(1024)} %param.22) | copy-start | bytes 18436
  198.6 2.8 copy-start.4
  198.6 223.7 %collective-permute-start.2 = (bf16[1,1536]{1,0:T(2,128)(2,1)S(1)}, bf16[1,1536]{1,0:T(2,128)(2,1)S(1)}, u32[]{:S(2)}, u32[]{:S(2)}) collective-permute-start(bf16[1,1536]{1,0:T(2,128)(2,1)S(1)} %get-tuple-element.10), channel_id=1, source_target_pairs={{0,4},{4,8},{8,12},{1,5},{5,9},{9,13},{2,6},{6,10},{10,14},{3,7},{... | collective-permute-start | bytes 9224 | tf_op jit(solution)/shard_map/ppermute | solution.py:21
  199.9 222.4 %collective-permute-start.3 = (bf16[1,1536]{1,0:T(2,128)(2,1)S(1)}, bf16[1,1536]{1,0:T(2,128)(2,1)S(1)}, u32[]{:S(2)}, u32[]{:S(2)}) collective-permute-start(bf16[1,1536]{1,0:T(2,128)(2,1)S(1)} %get-tuple-element.11), channel_id=1, source_target_pairs={{4,0},{8,4},{12,8},{5,1},{9,5},{13,9},{6,2},{10,6},{14,10},{7,3},{... | collective-permute-start | bytes 9224 | tf_op jit(solution)/shard_map/ppermute | solution.py:23
Sparse Core Ops, SparseCore 0:
  22.4 16.9 all-gather.5
  40.9 34.4 all-gather.7
  77.0 115.3 all-gather.9
  193.8 113.5 all-gather.11
  308.8 113.4 all-gather.13
  437.7 29.3 reduce-scatter.1
where the time goes:
time: 476 us
  waiting for transfers between devices  418 us (88%)
  matrix products  29.4 us (6%)
  between operations  13.7 us (3%)
  starting transfers between devices  9.21 us (2%)
    all_gather x1, waiting for transfers between devices, shards(): lax.all_gather(w_down, 'sp', axis=1, tiled=True)  115 us
    all_gather x1, waiting for transfers between devices, shards(): lax.all_gather(w_gate, 'sp', axis=0, tiled=True)  111 us
    all_gather x1, waiting for transfers between devices, shards(): lax.all_gather(w_up, 'sp', axis=0, tiled=True)  106 us
    all_gather x1, waiting for transfers between devices, shards(): full_proj = lax.all_gather(out_proj, 'tp', axis=1, tiled=True)  36 us
    reduce_scatter x1, waiting for transfers between devices, shards(): lax.psum_scatter(terms.astype(jnp.bfloat16), 'tp', scatter_dimension=1, t...  29.5 us
    dot_general x1, matrix products, shards(): jnp.dot(act, lax.all_gather(w_down, 'sp', axis=1, tiled=True), preferred_...  15.3 us
    all_gather x1, waiting for transfers between devices, shards(): all_heads = lax.all_gather(heads_out, 'tp', axis=1, tiled=True)  14.4 us
  transfers between devices with their start and end apart: 10, of which 7 were waited for; matrix products, arithmetic and copies ran while one was open for 3% of the time, Pallas kernels for 0%

commit v1 on v0

--- a/solution.py
+++ b/solution.py
@@ -1,6 +1,10 @@
+import functools
+
 import jax
 import jax.numpy as jnp
 from jax import lax
+from jax.experimental import pallas as pl
+from jax.experimental.pallas import tpu as pltpu
 from jax.sharding import PartitionSpec as P
 
 H = 8
@@ -99,9 +103,449 @@
     return (normed_own.astype(jnp.float32) + ffn_own).astype(jnp.bfloat16)
 
 
+CHUNKS = 2
+PAD = 8
+EDGE = 16
+BF16 = jnp.bfloat16
+F32 = jnp.float32
+
+
+def layer_kernel(
+    sizes,
+    q_ref, k_ref, v_ref, sink_ref, resid_ref, proj_ref, gain_ref, wg_ref, wu_ref, cw_ref, cb_ref, wd_ref,
+    out_ref,
+    kv_ext, proj_all, mixed, summed, normed, wg_all, wu_all, wd_all, gate, up, edge, halo, act, terms, parts,
+    halo_send, halo_recv, z_recv, right_send, left_send, y_recv, y_send,
+    proj_send, proj_recv, mix_send, mix_recv, edge_send, edge_recv, term_send, term_recv,
+):
+    groups, n, tps = sizes
+    g = lax.axis_index("grp")
+    s = lax.axis_index("sp")
+    t = lax.axis_index("tp")
+    tokens, width = resid_ref.shape
+    heads_here = sink_ref.shape[0]
+    cols = proj_ref.shape[1]
+    depth = wg_ref.shape[0]
+    hidden = wg_ref.shape[1]
+    has_left, has_right = s > 0, s < n - 1
+    own = (wg_ref, wu_ref, wd_ref)
+    full = (wg_all, wu_all, wd_all)
+
+    def remote(src, dst, send, recv, to):
+        return pltpu.make_async_remote_copy(
+            src_ref=src, dst_ref=dst, send_sem=send, recv_sem=recv,
+            device_id=to, device_id_type=pl.DeviceIdType.MESH,
+        )
+
+    barrier = pltpu.get_barrier_semaphore()
+
+    def greet(to):
+        pl.semaphore_signal(barrier, inc=1, device_id=to, device_id_type=pl.DeviceIdType.MESH)
+
+    @pl.when(has_left)
+    def _():
+        greet({"sp": s - 1})
+
+    @pl.when(has_right)
+    def _():
+        greet({"sp": s + 1})
+
+    for j in range(1, groups):
+        greet({"grp": lax.rem(g + j, groups)})
+    for j in range(1, tps):
+        greet({"tp": lax.rem(t + j, tps)})
+
+    along = jnp.minimum(s, 1) + jnp.minimum(n - 1 - s, 1)
+    pl.semaphore_wait(barrier, along + groups - 1 + tps - 1)
+
+    kv_head = (t * heads_here) // (H // KVH)
+    kv_cols = pl.ds(pl.multiple_of(kv_head * HD, HD), HD)
+
+    def halo_copy(i, to_left):
+        ref = (k_ref, v_ref)[i]
+        if to_left:
+            return remote(ref.at[pl.ds(0, WINDOW), kv_cols], kv_ext.at[i, pl.ds(WINDOW + tokens, WINDOW)],
+                          halo_send.at[i, 0], halo_recv.at[i, 0], {"sp": s - 1})
+        return remote(ref.at[pl.ds(tokens - WINDOW, WINDOW), kv_cols], kv_ext.at[i, pl.ds(0, WINDOW)],
+                      halo_send.at[i, 1], halo_recv.at[i, 1], {"sp": s + 1})
+
+    def rows_of(m, part, c):
+        step = own[m].shape[0] // (groups * CHUNKS)
+        return pl.ds(pl.multiple_of((part * CHUNKS + c) * step, EDGE), step)
+
+    def hop(m, p, c, side, is_own):
+        rows = rows_of(m, g, c)
+        src = own[m].at[rows] if is_own else full[m].at[p, rows]
+        sem = (right_send, left_send)[side].at[m, p, c]
+        return remote(src, full[m].at[p, rows], sem, z_recv.at[m, p, c], {"sp": (s + 1, s - 1)[side]})
+
+    def cross(m, p, c, j):
+        rows = rows_of(m, g, c)
+        return remote(full[m].at[p, rows], full[m].at[p, rows], y_send.at[m, p, c, j],
+                      y_recv.at[m, p, c, j], {"grp": lax.rem(g + j, groups)})
+
+    def cross_arrival(m, p, c, j):
+        rows = rows_of(m, lax.rem(g + groups - j, groups), c)
+        return remote(full[m].at[p, rows], full[m].at[p, rows], y_send.at[m, p, c, j],
+                      y_recv.at[m, p, c, j], {"grp": lax.rem(g + j, groups)})
+
+    def proj_copy(j):
+        return remote(proj_ref, proj_all.at[t], proj_send.at[j], proj_recv.at[j], {"tp": lax.rem(t + j, tps)})
+
+    def proj_arrival(j):
+        return remote(proj_ref, proj_all.at[lax.rem(t + tps - j, tps)], proj_send.at[j], proj_recv.at[j],
+                      {"tp": lax.rem(t + j, tps)})
+
+    def mix_copy(j):
+        return remote(mixed.at[t], mixed.at[t], mix_send.at[j], mix_recv.at[j], {"tp": lax.rem(t + j, tps)})
+
+    def mix_arrival(j):
+        return remote(mixed.at[t], mixed.at[lax.rem(t + tps - j, tps)], mix_send.at[j], mix_recv.at[j],
+                      {"tp": lax.rem(t + j, tps)})
+
+    sides = ((has_right, 0), (has_left, 1))
+
+    @pl.when(has_left)
+    def _():
+        for i in range(2):
+            halo_copy(i, True).start()
+
+    @pl.when(has_right)
+    def _():
+        for i in range(2):
+            halo_copy(i, False).start()
+
+    for m in range(3):
+        for c in range(CHUNKS):
+            for able, side in sides:
+                @pl.when(able)
+                def _(m=m, c=c, side=side):
+                    hop(m, s, c, side, True).start()
+    for j in range(1, tps):
+        proj_copy(j).start()
+
+    for i, ref in enumerate((k_ref, v_ref)):
+        kv_ext[i, pl.ds(WINDOW, tokens), :] = ref[:, kv_cols]
+
+    @pl.when(jnp.logical_not(has_left))
+    def _():
+        kv_ext[:, pl.ds(0, WINDOW), :] = jnp.zeros((2, WINDOW, HD), BF16)
+
+    @pl.when(jnp.logical_not(has_right))
+    def _():
+        kv_ext[:, pl.ds(WINDOW + tokens, WINDOW), :] = jnp.zeros((2, WINDOW, HD), BF16)
+
+    @pl.when(has_right)
+    def _():
+        for i in range(2):
+            halo_copy(i, True).wait_recv()
+
+    @pl.when(has_left)
+    def _():
+        for i in range(2):
+            halo_copy(i, False).wait_recv()
+
+    span = 3 * WINDOW
+    seq_total = tokens * n
+
+    @pl.loop(0, tokens // WINDOW)
+    def _(b):
+        start = pl.multiple_of(b * WINDOW, WINDOW)
+        row = lax.broadcasted_iota(jnp.int32, (WINDOW, span), 0)
+        col = lax.broadcasted_iota(jnp.int32, (WINDOW, span), 1)
+        k_pos = s * tokens + start - WINDOW + col
+        valid = (jnp.abs(row + WINDOW - col) <= WINDOW) & (k_pos >= 0) & (k_pos < seq_total)
+        kb = kv_ext[0, pl.ds(start, span), :]
+        vb = kv_ext[1, pl.ds(start, span), :]
+        for h in range(heads_here):
+            qb = q_ref[pl.ds(start, WINDOW), h * HD:(h + 1) * HD]
+            sc = lax.dot_general(qb, kb, (((1,), (1,)), ((), ())), preferred_element_type=F32) * (HD ** -0.5)
+            sc = jnp.where(valid, sc, F32(-1e30))
+            sink = sink_ref[h]
+            top = jnp.maximum(jnp.max(sc, axis=-1, keepdims=True), sink)
+            expo = jnp.exp(sc - top)
+            total = jnp.sum(expo, axis=-1, keepdims=True) + jnp.exp(sink - top)
+            weights = (expo / total).astype(BF16)
+            o = jnp.dot(weights, vb, preferred_element_type=F32)
+            mixed[t, pl.ds(start, WINDOW), h * HD:(h + 1) * HD] = o.astype(BF16)
+
+    proj_all[t] = proj_ref[...]
+    for j in range(1, tps):
+        mix_copy(j).start()
+
+    def relay(k):
+        for m in range(3):
+            for c in range(CHUNKS):
+                for side in range(2):
+                    p = s - k if side == 0 else s + k
+                    here = p >= 0 if side == 0 else p < n
+                    able = sides[side][0]
+
+                    @pl.when(here)
+                    def _(m=m, c=c, side=side, p=p, able=able):
+                        hop(m, p, c, side, False).wait_recv()
+                        for j in range(1, groups):
+                            cross(m, p, c, j).start()
+                        if k < n - 1:
+                            @pl.when(able)
+                            def _():
+                                hop(m, p, c, side, False).start()
+
+    def arrived(m, p):
+        for c in range(CHUNKS):
+            for j in range(1, groups):
+                cross_arrival(m, p, c, j).wait_recv()
+
+    tile = cols
+
+    def gate_up(p, first):
+        x = normed[:, pl.ds(pl.multiple_of(p * depth, 128), depth)]
+
+        @pl.loop(0, hidden // tile)
+        def _(i):
+            at = pl.ds(pl.multiple_of(i * tile, 128), tile)
+            a = wg_ref[:, at] if first else wg_all[p, :, at]
+            ga = jnp.dot(x, a, preferred_element_type=F32)
+            b = wu_ref[:, at] if first else wu_all[p, :, at]
+            ub = jnp.dot(x, b, preferred_element_type=F32)
+            if first:
+                gate[pl.ds(PAD, tokens), at] = ga
+                up[:, at] = ub
+            else:
+                gate[pl.ds(PAD, tokens), at] += ga
+                up[:, at] += ub
+
+    def pieces(k, do):
+        @pl.loop(0, 2)
+        def _(side):
+            p = s + (2 * side - 1) * k
+
+            @pl.when((p >= 0) & (p < n))
+            def _():
+                do(p)
+
+    def gate_up_from(k):
+        def do(p):
+            arrived(0, p)
+            arrived(1, p)
+            gate_up(p, False)
+        pieces(k, do)
+
+    relay(1)
+
+    for j in range(1, tps):
+        proj_arrival(j).wait_recv()
+        mix_arrival(j).wait_recv()
+    lanes = mixed.shape[2]
+
+    @pl.loop(0, tps)
+    def _(i):
+        at = pl.ds(pl.multiple_of(i * cols, 128), cols)
+        total = resid_ref[:, at].astype(F32)
+        prod = jnp.dot(mixed[0], proj_all[i, pl.ds(0, lanes), :], preferred_element_type=F32)
+        for u in range(1, tps):
+            prod += jnp.dot(mixed[u], proj_all[i, pl.ds(u * lanes, lanes), :], preferred_element_type=F32)
+        summed[:, at] = total + prod
+
+    block = 64
+
+    @pl.loop(0, tokens // block)
+    def _(b):
+        at = pl.ds(pl.multiple_of(b * block, block), block)
+        x = summed[at, :]
+        mean = jnp.mean(x, axis=-1, keepdims=True)
+        msq = jnp.mean(x * x, axis=-1, keepdims=True)
+        normed[at, :] = ((x - mean) * lax.rsqrt(msq - mean * mean + 1e-05) * gain_ref[...]).astype(BF16)
+
+    gate_up(s, True)
+    for k in range(2, n):
+        relay(k)
+        gate_up_from(k - 1)
+    gate_up_from(n - 1)
+
+    edge[0] = gate[pl.ds(PAD, EDGE), :].astype(BF16)
+    edge[1] = gate[pl.ds(PAD + tokens - EDGE, EDGE), :].astype(BF16)
+
+    def edge_copy(to_left):
+        if to_left:
+            return remote(edge.at[0], halo.at[1], edge_send.at[0], edge_recv.at[1], {"sp": s - 1})
+        return remote(edge.at[1], halo.at[0], edge_send.at[1], edge_recv.at[0], {"sp": s + 1})
+
+    @pl.when(has_left)
+    def _():
+        edge_copy(True).start()
+
+    @pl.when(has_right)
+    def _():
+        edge_copy(False).start()
+
+    strip = 128
+
+    @pl.loop(0, hidden // strip)
+    def _(i):
+        at = pl.ds(pl.multiple_of(i * strip, strip), strip)
+        gate[pl.ds(PAD, tokens), at] = gate[pl.ds(PAD, tokens), at].astype(BF16).astype(F32)
+
+    gate[PAD - 1:PAD, :] = jnp.zeros((1, hidden), F32)
+    gate[PAD + tokens:PAD + tokens + 1, :] = jnp.zeros((1, hidden), F32)
+
+    @pl.when(has_left)
+    def _():
+        edge_copy(False).wait_recv()
+        gate[PAD - 1:PAD, :] = halo[0].astype(F32)[EDGE - 1:EDGE, :]
+
+    @pl.when(has_right)
+    def _():
+        edge_copy(True).wait_recv()
+        gate[PAD + tokens:PAD + tokens + 1, :] = halo[1].astype(F32)[0:1, :]
+
+    @pl.loop(0, hidden // strip)
+    def _(i):
+        at = pl.ds(pl.multiple_of(i * strip, strip), strip)
+        conv = cb_ref[:, at]
+        for tap in range(CONV):
+            conv = conv + gate[pl.ds(PAD - CONV // 2 + tap, tokens), at] * cw_ref[tap:tap + 1, at]
+        silu = conv / (1.0 + jnp.exp(-conv))
+        act[:, at] = (silu * up[:, at].astype(BF16).astype(F32)).astype(BF16)
+
+    def term_copy(p):
+        return remote(terms.at[p], parts.at[t], term_send.at[p], term_recv.at[t], {"tp": p})
+
+    def down(p, first):
+        @pl.loop(0, cols // 256)
+        def _(i):
+            at = pl.ds(pl.multiple_of(i * 256, 256), 256)
+            w = wd_ref[:, at] if first else wd_all[p, :, at]
+            terms[p, :, at] = jnp.dot(act[...], w, preferred_element_type=F32).astype(BF16)
+
+        @pl.when(p != t)
+        def _():
+            term_copy(p).start()
+
+    down(s, True)
+    for k in range(1, n):
+        def do(p):
+            arrived(2, p)
+            down(p, False)
+        pieces(k, do)
+
+    out = normed[:, pl.ds(pl.multiple_of(t * cols, 128), cols)].astype(F32) + terms[t].astype(F32)
+    for j in range(1, tps):
+        u = lax.rem(t + j, tps)
+        remote(terms.at[u], parts.at[u], term_send.at[u], term_recv.at[u], {"tp": u}).wait_recv()
+    for j in range(1, tps):
+        out = out + parts[lax.rem(t + j, tps)].astype(F32)
+    out_ref[...] = out.astype(BF16)
+
+    @pl.when(has_left)
+    def _():
+        for i in range(2):
+            halo_copy(i, True).wait_send()
+        edge_copy(True).wait_send()
+
+    @pl.when(has_right)
+    def _():
+        for i in range(2):
+            halo_copy(i, False).wait_send()
+        edge_copy(False).wait_send()
+
+    for j in range(1, tps):
+        proj_copy(j).wait_send()
+        mix_copy(j).wait_send()
+        term_copy(lax.rem(t + j, tps)).wait_send()
+    for m in range(3):
+        for c in range(CHUNKS):
+            for able, side in sides:
+                @pl.when(able)
+                def _(m=m, c=c, side=side):
+                    hop(m, s, c, side, True).wait_send()
+            for k in range(1, n):
+                for side in range(2):
+                    p = s - k if side == 0 else s + k
+                    here = p >= 0 if side == 0 else p < n
+
+                    @pl.when(here)
+                    def _(m=m, c=c, side=side, p=p):
+                        for j in range(1, groups):
+                            cross(m, p, c, j).wait_send()
+                        if k < n - 1:
+                            @pl.when(sides[side][0])
+                            def _():
+                                hop(m, p, c, side, False).wait_send()
+
+
+def kernel_shards(
+    sizes, queries, keys, values, sink, resid, out_proj, norm_gain, w_gate, w_up, conv_w, conv_b, w_down
+):
+    groups, n, tps = sizes
+    tokens, width = resid.shape
+    cols = out_proj.shape[1]
+    depth, hidden = w_gate.shape
+    vmem = pl.BlockSpec(memory_space=pltpu.VMEM)
+    dma = pltpu.SemaphoreType.DMA
+    shard_sems = dma((3, n, CHUNKS))
+    cross_sems = dma((3, n, CHUNKS, groups))
+    return pl.pallas_call(
+        functools.partial(layer_kernel, sizes),
+        out_shape=jax.ShapeDtypeStruct((tokens, cols), BF16),
+        in_specs=[vmem] * 3 + [pl.BlockSpec(memory_space=pltpu.SMEM)] + [vmem] * 8,
+        out_specs=vmem,
+        scratch_shapes=[
+            pltpu.VMEM((2, tokens + 2 * WINDOW, HD), BF16),
+            pltpu.VMEM((tps,) + out_proj.shape, BF16),
+            pltpu.VMEM((tps,) + queries.shape, BF16),
+            pltpu.VMEM((tokens, width), F32),
+            pltpu.VMEM((tokens, width), BF16),
+            pltpu.VMEM((n,) + w_gate.shape, BF16),
+            pltpu.VMEM((n,) + w_up.shape, BF16),
+            pltpu.VMEM((n,) + w_down.shape, BF16),
+            pltpu.VMEM((tokens + 2 * PAD, hidden), F32),
+            pltpu.VMEM((tokens, hidden), F32),
+            pltpu.VMEM((2, EDGE, hidden), BF16),
+            pltpu.VMEM((2, EDGE, hidden), BF16),
+            pltpu.VMEM((tokens, hidden), BF16),
+            pltpu.VMEM((tps, tokens, cols), BF16),
+            pltpu.VMEM((tps, tokens, cols), BF16),
+            dma((2, 2)), dma((2, 2)),
+            shard_sems, shard_sems, shard_sems, cross_sems, cross_sems,
+            dma((tps,)), dma((tps,)), dma((tps,)), dma((tps,)),
+            dma((2,)), dma((2,)), dma((tps,)), dma((tps,)),
+        ],
+        compiler_params=pltpu.CompilerParams(
+            collective_id=0, has_side_effects=True, vmem_limit_bytes=64 * 1000 * 1000
+        ),
+    )(queries, keys, values, sink, resid, out_proj, norm_gain[None], w_gate, w_up, conv_w, conv_b[None], w_down)
+
+
+def fits_kernel(sizes, args):
+    groups, n, tps = sizes
+    queries, resid, out_proj, w_gate, w_down = args[0], args[4], args[5], args[7], args[11]
+    part = groups * CHUNKS * EDGE
+    weights = 3 * 2 * n * w_gate.shape[0] * w_gate.shape[1]
+    return (
+        n == tps
+        and n > 1
+        and groups > 1
+        and w_down.shape[1] == out_proj.shape[1]
+        and w_gate.shape[0] % max(part, 128) == 0
+        and w_down.shape[0] % part == 0
+        and w_down.shape[1] % 256 == 0
+        and w_gate.shape[1] % out_proj.shape[1] == 0
+        and resid.shape[0] % WINDOW == 0
+        and weights <= 20 * 2 ** 20
+    )
+
+
+def run_shards(sizes, *args):
+    if fits_kernel(sizes, args):
+        return kernel_shards(sizes, *args)
+    return shards(*args)
+
+
 def solution(mesh):
+    sizes = tuple(mesh.shape[axis] for axis in ("grp", "sp", "tp"))
     return jax.shard_map(
-        shards,
+        functools.partial(run_shards, sizes),
         mesh=mesh,
         in_specs=(
             P(("grp", "sp"), "tp"),

time: 476 us -> 203 us (0.43)
  waiting for transfers between devices: 418 us -> 0 us
  Pallas kernels: 0 us -> 199 us
  matrix products: 29.4 us -> 0 us
  between operations: 13.7 us -> 0.01 us
  starting transfers between devices: 9.21 us -> 0 us
    all_gather x5 -> x0, waiting for transfers between devices: 382 us -> none  [the longest x1 115 us: shards(): lax.all_gather(w_down, 'sp', axis=1, tiled=True)]
    pallas_call x0 -> x1, Pallas kernels: none -> 199 us  [kernel_shards(): pl.pallas_call(functools.partial(layer_kernel, sizes), out_shape=jax.Shap...]
    reduce_scatter x1 -> x0, waiting for transfers between devices: 29.5 us -> none  [shards(): lax.psum_scatter(terms.astype(jnp.bfloat16), 'tp', scatter_dimension=1, t...]
    dot_general x5 -> x0, matrix products: 29.4 us -> none  [the longest x1 15.3 us: shards(): jnp.dot(act, lax.all_gather(w_down, 'sp', axis=1, tiled=True), preferred_...]
    ppermute x4 -> x0, starting transfers between devices: 9.01 us -> none  [the longest x2 6.25 us: with_halo(): lax.ppermute(tail, axis, [(i, (i + 1) % count) for i in range(ends)])]
  transfers between devices with their start and end apart: 10 -> 0, of which waited for: 7 -> 0; matrix products, arithmetic and copies ran while one was open for 3% -> 0% of each run, Pallas kernels for 0% -> 0%
where the time goes in v1:
time: 203 us; the launch traced here: 202 us
  Pallas kernels  199 us (98%)
  local copies, waits for them, and re-layouts  3.16 us (2%)
    pallas_call x1, Pallas kernels, kernel_shards(): pl.pallas_call(functools.partial(layer_kernel, sizes), out_shape=jax.Shap...  199 us

profile of v1, /device:TPU:0, one launch (start us, length us, event | category | flops | bytes accessed | tf_op | source)
XLA Modules:
  0.0 202.0 jit_solution(3924566694063187623)
XLA Ops:
  0.0 1.3 broadcast_in_dim.7.cb_ref
  1.3 198.8 %shard_map.118 = bf16[512,512]{1,0:T(8,128)(2,1)} custom-call(bf16[512,256]{1,0:T(8,128)(2,1)} %q_ref.1, bf16[512,256]{1,0:T(8,128)(2,1)} %k_ref.1, bf16[512,256]{1,0:T(8,128)(2,1)} %v_ref.1, f32[2]{0:T(128)} %sink_ref.1, bf16[512,2048]{1,0:T(8,128)(2,1)} %resid_ref.1, bf16[1024,512]{1,0:T(8,128)(2,1)} %proj_ref.1, f32[1,2048]{1,0:T(1,128)} %bitcast.1, ...), custom_call_target="tpu_custom_call" | custom-call | tf_op jit(solution)/shard_map/pallas_call | solution.py:488
  200.1 1.9 copy.14

commit v2 on v0

--- a/solution.py
+++ b/solution.py
@@ -1,6 +1,10 @@
+import functools
+
 import jax
 import jax.numpy as jnp
 from jax import lax
+from jax.experimental import pallas as pl
+from jax.experimental.pallas import tpu as pltpu
 from jax.sharding import PartitionSpec as P
 
 H = 8
@@ -99,9 +103,504 @@
     return (normed_own.astype(jnp.float32) + ffn_own).astype(jnp.bfloat16)
 
 
+CHUNKS = 2
+CROSSED = 1
+PAD = 8
+EDGE = 16
+BF16 = jnp.bfloat16
+F32 = jnp.float32
+
+
+def layer_kernel(
+    sizes,
+    q_ref, k_ref, v_ref, sink_ref, resid_ref, proj_ref, gain_ref, wg_ref, wu_ref, cw_ref, cb_ref, wd_ref,
+    out_ref,
+    kv_ext, proj_all, mixed, summed, normed, wg_all, wu_all, wd_all, gate, up, edge, halo, act, terms, parts,
+    ret_out, ret_in,
+    halo_send, halo_recv, z_recv, z_send, y_recv, y_send,
+    proj_send, proj_recv, mix_send, mix_recv, norm_send, norm_recv, edge_send, edge_recv,
+    term_send, term_recv, ret_send, ret_recv,
+):
+    groups, n, tps = sizes
+    g = lax.axis_index("grp")
+    s = lax.axis_index("sp")
+    t = lax.axis_index("tp")
+    tokens, width = resid_ref.shape
+    heads_here = sink_ref.shape[0]
+    cols = proj_ref.shape[1]
+    depth = wg_ref.shape[0]
+    hidden = wg_ref.shape[1]
+    rows2 = 2 * tokens
+    has_left, has_right = s > 0, s < n - 1
+    inner = has_left & has_right
+    outer = jnp.logical_not(inner)
+    low = s < n // 2
+    inward = 1 - 2 * (s // (n // 2))
+    base = pl.multiple_of(lax.rem(s, 2) * tokens, tokens)
+    other_base = pl.multiple_of((1 - lax.rem(s, 2)) * tokens, tokens)
+    core_peer = t + 1 - 2 * lax.rem(t, 2)
+    chip_peer = lax.rem(t + 2, tps)
+    own = (wg_ref, wu_ref, wd_ref)
+    full = (wg_all, wu_all, wd_all)
+
+    def remote(src, dst, send, recv, to):
+        return pltpu.make_async_remote_copy(
+            src_ref=src, dst_ref=dst, send_sem=send, recv_sem=recv,
+            device_id=to, device_id_type=pl.DeviceIdType.MESH,
+        )
+
+    barrier = pltpu.get_barrier_semaphore()
+
+    def greet(to):
+        pl.semaphore_signal(barrier, inc=1, device_id=to, device_id_type=pl.DeviceIdType.MESH)
+
+    @pl.when(has_left)
+    def _():
+        greet({"sp": s - 1})
+
+    @pl.when(has_right)
+    def _():
+        greet({"sp": s + 1})
+
+    for j in range(1, groups):
+        greet({"grp": lax.rem(g + j, groups)})
+    for j in range(1, tps):
+        greet({"tp": lax.rem(t + j, tps)})
+    along = jnp.minimum(s, 1) + jnp.minimum(n - 1 - s, 1)
+    pl.semaphore_wait(barrier, along + groups - 1 + tps - 1)
+
+    kv_head = (t * heads_here) // (H // KVH)
+    kv_cols = pl.ds(pl.multiple_of(kv_head * HD, HD), HD)
+
+    def halo_copy(i, to_left):
+        ref = (k_ref, v_ref)[i]
+        if to_left:
+            return remote(ref.at[pl.ds(0, WINDOW), kv_cols], kv_ext.at[i, pl.ds(WINDOW + tokens, WINDOW)],
+                          halo_send.at[i, 0], halo_recv.at[i, 0], {"sp": s - 1})
+        return remote(ref.at[pl.ds(tokens - WINDOW, WINDOW), kv_cols], kv_ext.at[i, pl.ds(0, WINDOW)],
+                      halo_send.at[i, 1], halo_recv.at[i, 1], {"sp": s + 1})
+
+    def rows_of(m, part, c):
+        step = own[m].shape[0] // (groups * CHUNKS)
+        return pl.ds(pl.multiple_of((part * CHUNKS + c) * step, EDGE), step)
+
+    def hop(m, src_slot, dst_slot, j, c):
+        part = lax.rem(g + j, groups)
+        rows = rows_of(m, part, c)
+        src = own[m].at[rows] if src_slot is None else full[m].at[src_slot, rows]
+        return remote(src, full[m].at[dst_slot, rows], z_send.at[m, 0 if src_slot is None else 1, j, c],
+                      z_recv.at[m, dst_slot, j, c], {"sp": s + inward})
+
+    def cross(m, slot, c, j):
+        rows = rows_of(m, g, c)
+        return remote(full[m].at[slot, rows], full[m].at[slot, rows], y_send.at[m, slot, c, j],
+                      y_recv.at[m, slot, c, j], {"grp": lax.rem(g + j, groups)})
+
+    def cross_arrival(m, slot, c, j):
+        rows = rows_of(m, lax.rem(g + groups - j, groups), c)
+        return remote(full[m].at[slot, rows], full[m].at[slot, rows], y_send.at[m, slot, c, j],
+                      y_recv.at[m, slot, c, j], {"grp": lax.rem(g + j, groups)})
+
+    pieces = [(m, c) for m in range(3) for c in range(CHUNKS)]
+    crossed = pieces[:CROSSED]
+    direct = [(m, c, j) for m, c in pieces[CROSSED:] for j in range(1, groups)]
+
+    def spread(src, ref, send, recv, step):
+        origin = (t, t, chip_peer)[step]
+        return remote(src if step < 2 else ref.at[origin], ref.at[origin], send.at[step], recv.at[step],
+                      {"tp": (core_peer, chip_peer, core_peer)[step]})
+
+    def spread_arrival(src, ref, send, recv, step):
+        origin = (core_peer, chip_peer, lax.rem(core_peer + 2, tps))[step]
+        return remote(src, ref.at[origin], send.at[step], recv.at[step],
+                      {"tp": (core_peer, chip_peer, core_peer)[step]})
+
+    proj_args = (proj_ref, proj_all, proj_send, proj_recv)
+    mix_args = (mixed.at[t], mixed, mix_send, mix_recv)
+
+    @pl.when(has_left)
+    def _():
+        for i in range(2):
+            halo_copy(i, True).start()
+
+    @pl.when(has_right)
+    def _():
+        for i in range(2):
+            halo_copy(i, False).start()
+
+    @pl.when(outer)
+    def _():
+        for m, c in pieces:
+            hop(m, None, 0, 0, c).start()
+
+    @pl.when(inner)
+    def _():
+        for m, c in pieces:
+            hop(m, None, 1, 0, c).start()
+
+    for step in (1, 0):
+        spread(*proj_args, step).start()
+
+    for i, ref in enumerate((k_ref, v_ref)):
+        kv_ext[i, pl.ds(WINDOW, tokens), :] = ref[:, kv_cols]
+
+    @pl.when(jnp.logical_not(has_left))
+    def _():
+        kv_ext[:, pl.ds(0, WINDOW), :] = jnp.zeros((2, WINDOW, HD), BF16)
+
+    @pl.when(jnp.logical_not(has_right))
+    def _():
+        kv_ext[:, pl.ds(WINDOW + tokens, WINDOW), :] = jnp.zeros((2, WINDOW, HD), BF16)
+
+    @pl.when(has_right)
+    def _():
+        for i in range(2):
+            halo_copy(i, True).wait_recv()
+
+    @pl.when(has_left)
+    def _():
+        for i in range(2):
+            halo_copy(i, False).wait_recv()
+
+    span = 3 * WINDOW
+    seq_total = tokens * n
+
+    @pl.loop(0, tokens // WINDOW)
+    def _(b):
+        start = pl.multiple_of(b * WINDOW, WINDOW)
+        row = lax.broadcasted_iota(jnp.int32, (WINDOW, span), 0)
+        col = lax.broadcasted_iota(jnp.int32, (WINDOW, span), 1)
+        k_pos = s * tokens + start - WINDOW + col
+        valid = (jnp.abs(row + WINDOW - col) <= WINDOW) & (k_pos >= 0) & (k_pos < seq_total)
+        kb = kv_ext[0, pl.ds(start, span), :]
+        vb = kv_ext[1, pl.ds(start, span), :]
+        for h in range(heads_here):
+            qb = q_ref[pl.ds(start, WINDOW), h * HD:(h + 1) * HD]
+            sc = lax.dot_general(qb, kb, (((1,), (1,)), ((), ())), preferred_element_type=F32) * (HD ** -0.5)
+            sc = jnp.where(valid, sc, F32(-1e30))
+            sink = sink_ref[h]
+            top = jnp.maximum(jnp.max(sc, axis=-1, keepdims=True), sink)
+            expo = jnp.exp(sc - top)
+            total = jnp.sum(expo, axis=-1, keepdims=True) + jnp.exp(sink - top)
+            weights = (expo / total).astype(BF16)
+            o = jnp.dot(weights, vb, preferred_element_type=F32)
+            mixed[t, pl.ds(start, WINDOW), h * HD:(h + 1) * HD] = o.astype(BF16)
+
+    proj_all[t] = proj_ref[...]
+    for step in (1, 0):
+        spread(*mix_args, step).start()
+
+    def relay_near(m):
+        for c in range(CHUNKS):
+            hop(m, None, 0, 0, c).wait_recv()
+            hop(m, 0, 2, 0, c).start()
+            if (m, c) in crossed:
+                for j in range(1, groups):
+                    cross(m, 0, c, j).start()
+            hop(m, None, 1, 0, c).wait_recv()
+            for j in range(1, groups):
+                cross(m, 1, c, j).start()
+
+    def relay_far(m):
+        for c in range(CHUNKS):
+            hop(m, 0, 2, 0, c).wait_recv()
+            for j in range(1, groups):
+                cross(m, 2, c, j).start()
+
+    @pl.when(inner)
+    def _():
+        relay_near(0)
+
+    for args in (proj_args, mix_args):
+        spread_arrival(*args, 1).wait_recv()
+        spread(*args, 2).start()
+    for args in (proj_args, mix_args):
+        for step in (0, 2):
+            spread_arrival(*args, step).wait_recv()
+    lanes = mixed.shape[2]
+    block = summed.shape[0]
+    strip = 64
+
+    @pl.loop(0, tokens // block)
+    def _(b):
+        rows = pl.ds(pl.multiple_of(b * block, block), block)
+
+        @pl.loop(0, tps)
+        def _(i):
+            at = pl.ds(pl.multiple_of(i * cols, 128), cols)
+            prod = jnp.dot(mixed[0, rows, :], proj_all[i, pl.ds(0, lanes), :], preferred_element_type=F32)
+            for u in range(1, tps):
+                prod += jnp.dot(mixed[u, rows, :], proj_all[i, pl.ds(u * lanes, lanes), :],
+                                preferred_element_type=F32)
+            summed[:, at] = resid_ref[rows, at].astype(F32) + prod
+
+        @pl.loop(0, block // strip)
+        def _(i):
+            at = pl.multiple_of(i * strip, strip)
+            x = summed[pl.ds(at, strip), :]
+            mean = jnp.mean(x, axis=-1, keepdims=True)
+            msq = jnp.mean(x * x, axis=-1, keepdims=True)
+            normed[pl.ds(pl.multiple_of(base + b * block + at, strip), strip), :] = (
+                (x - mean) * lax.rsqrt(msq - mean * mean + 1e-05) * gain_ref[...]
+            ).astype(BF16)
+
+    half = width // 2
+    my_half = pl.ds(pl.multiple_of(lax.rem(t, 2) * half, half), half)
+    peer_half = pl.ds(pl.multiple_of((1 - lax.rem(t, 2)) * half, half), half)
+
+    def norm_in():
+        part = normed.at[pl.ds(base, tokens), my_half]
+        return remote(part, part, norm_send.at[0], norm_recv.at[0], {"sp": s + inward})
+
+    def norm_in_arrival():
+        part = normed.at[pl.ds(other_base, tokens), my_half]
+        return remote(part, part, norm_send.at[0], norm_recv.at[0], {"sp": s + inward})
+
+    def norm_over(of_peer):
+        part = normed.at[pl.ds(other_base, tokens), peer_half if of_peer else my_half]
+        return remote(part, part, norm_send.at[1], norm_recv.at[1], {"tp": core_peer})
+
+    def ret_copy():
+        return remote(ret_out, ret_in, ret_send.at[0], ret_recv.at[0], {"sp": s - inward})
+
+    def edge_copy():
+        return remote(edge, halo, edge_send.at[0], edge_recv.at[0], {"sp": s + inward})
+
+    def term_copy(p, own_rows):
+        rows = pl.ds(base if own_rows else other_base, tokens)
+        i = int(own_rows)
+        return remote(terms.at[p, rows], parts.at[t, rows], term_send.at[p, i], term_recv.at[t, i], {"tp": p})
+
+    def term_arrival(u, own_rows):
+        rows = pl.ds(base if own_rows else other_base, tokens)
+        i = int(own_rows)
+        return remote(terms.at[u, rows], parts.at[u, rows], term_send.at[u, i], term_recv.at[u, i], {"tp": u})
+
+    tile = 256
+    my_cols = pl.ds(pl.multiple_of(t * cols, 128), cols)
+
+    def arrived(m, slot):
+        for c in range(CHUNKS):
+            for j in range(1, groups):
+                if slot == 0 and (m, c) not in crossed:
+                    hop(m, None, 0, j, c).wait_recv()
+                else:
+                    cross_arrival(m, slot, c, j).wait_recv()
+
+    def gate_up(slot):
+        if slot is not None:
+            arrived(0, slot)
+            arrived(1, slot)
+        p = s + {None: 0, 0: -1, 1: 1, 2: 2}[slot] * inward
+
+        @pl.loop(0, hidden // tile)
+        def _(i):
+            at = pl.ds(pl.multiple_of(i * tile, 128), tile)
+            x = normed[:, pl.ds(pl.multiple_of(p * depth, 128), depth)]
+            wa = wg_ref[:, at] if slot is None else wg_all[slot, :, at]
+            ga = jnp.dot(x, wa, preferred_element_type=F32)
+            if slot is None:
+                gate[pl.ds(PAD, rows2), at] = ga
+            else:
+                gate[pl.ds(PAD, rows2), at] += ga
+            wb = wu_ref[:, at] if slot is None else wu_all[slot, :, at]
+            ub = jnp.dot(x, wb, preferred_element_type=F32)
+            if slot is None:
+                up[:, at] = ub
+            else:
+                up[:, at] += ub
+
+    def down(slot):
+        if slot is not None:
+            arrived(2, slot)
+        p = s + {None: 0, 0: -1, 1: 1, 2: 2}[slot] * inward
+        for own_rows in (False, True):
+            rows = pl.ds(base if own_rows else other_base, tokens)
+
+            @pl.loop(0, cols // tile)
+            def _(i):
+                at = pl.ds(pl.multiple_of(i * tile, 128), tile)
+                w = wd_ref[:, at] if slot is None else wd_all[slot, :, at]
+                terms[p, rows, at] = jnp.dot(act[rows, :], w, preferred_element_type=F32).astype(BF16)
+
+            @pl.when(p != t)
+            def _():
+                term_copy(p, own_rows).start()
+
+    def finish(own_rows):
+        rows = pl.ds(base if own_rows else other_base, tokens)
+        out = normed[rows, my_cols].astype(F32) + terms[t, rows, :].astype(F32)
+        for j in range(1, tps):
+            u = lax.rem(t + j, tps)
+            term_arrival(u, own_rows).wait_recv()
+            out = out + parts[u, rows, :].astype(F32)
+        return out.astype(BF16)
+
+    @pl.when(outer)
+    def _():
+        norm_in().start()
+        for m, c, j in direct:
+            hop(m, None, 0, j, c).start()
+        ret_copy().wait_recv()
+        out_ref[...] = ret_in[...]
+        norm_in().wait_send()
+        for m, c, j in direct:
+            hop(m, None, 0, j, c).wait_send()
+        for m, c in pieces:
+            hop(m, None, 0, 0, c).wait_send()
+
+    @pl.when(inner)
+    def _():
+        relay_near(1)
+        relay_near(2)
+        relay_far(0)
+        norm_in_arrival().wait_recv()
+        norm_over(False).start()
+        relay_far(1)
+        norm_over(True).wait_recv()
+        gate_up(None)
+        gate_up(1)
+        relay_far(2)
+        gate_up(0)
+        gate_up(2)
+
+        at_edge = pl.multiple_of(PAD + (1 - s // (n // 2)) * (rows2 - EDGE), PAD)
+        edge[...] = gate[pl.ds(at_edge, EDGE), :].astype(BF16)
+        edge_copy().start()
+        gate[PAD - 1:PAD, :] = jnp.zeros((1, hidden), F32)
+        gate[PAD + rows2:PAD + rows2 + 1, :] = jnp.zeros((1, hidden), F32)
+        edge_copy().wait_recv()
+
+        @pl.when(low)
+        def _():
+            gate[PAD + rows2:PAD + rows2 + 1, :] = halo[...].astype(F32)[0:1, :]
+
+        @pl.when(jnp.logical_not(low))
+        def _():
+            gate[PAD - 1:PAD, :] = halo[...].astype(F32)[EDGE - 1:EDGE, :]
+
+        @pl.loop(0, hidden // 128)
+        def _(i):
+            at = pl.ds(pl.multiple_of(i * 128, 128), 128)
+            gate[pl.ds(PAD, rows2), at] = gate[pl.ds(PAD, rows2), at].astype(BF16).astype(F32)
+            conv = cb_ref[:, at]
+            for tap in range(CONV):
+                conv = conv + gate[pl.ds(PAD - CONV // 2 + tap, rows2), at] * cw_ref[tap:tap + 1, at]
+            silu = conv / (1.0 + jnp.exp(-conv))
+            act[:, at] = (silu * up[:, at].astype(BF16).astype(F32)).astype(BF16)
+
+        down(None)
+        down(1)
+        down(2)
+        down(0)
+        ret_out[...] = finish(False)
+        ret_copy().start()
+        out_ref[...] = finish(True)
+
+        ret_copy().wait_send()
+        edge_copy().wait_send()
+        norm_over(False).wait_send()
+        for j in range(1, tps):
+            for own_rows in (False, True):
+                term_copy(lax.rem(t + j, tps), own_rows).wait_send()
+        for m, c in pieces:
+            hop(m, None, 1, 0, c).wait_send()
+            hop(m, 0, 2, 0, c).wait_send()
+            for j in range(1, groups):
+                if (m, c) in crossed:
+                    cross(m, 0, c, j).wait_send()
+                cross(m, 1, c, j).wait_send()
+                cross(m, 2, c, j).wait_send()
+
+    @pl.when(has_left)
+    def _():
+        for i in range(2):
+            halo_copy(i, True).wait_send()
+
+    @pl.when(has_right)
+    def _():
+        for i in range(2):
+            halo_copy(i, False).wait_send()
+
+    for step in range(3):
+        spread(*proj_args, step).wait_send()
+        spread(*mix_args, step).wait_send()
+
+
+def kernel_shards(
+    sizes, queries, keys, values, sink, resid, out_proj, norm_gain, w_gate, w_up, conv_w, conv_b, w_down
+):
+    groups, n, tps = sizes
+    tokens, width = resid.shape
+    cols = out_proj.shape[1]
+    depth, hidden = w_gate.shape
+    vmem = pl.BlockSpec(memory_space=pltpu.VMEM)
+    dma = pltpu.SemaphoreType.DMA
+    cross_sems = dma((3, 3, CHUNKS, groups))
+    return pl.pallas_call(
+        functools.partial(layer_kernel, sizes),
+        out_shape=jax.ShapeDtypeStruct((tokens, cols), BF16),
+        in_specs=[vmem] * 3 + [pl.BlockSpec(memory_space=pltpu.SMEM)] + [vmem] * 8,
+        out_specs=vmem,
+        scratch_shapes=[
+            pltpu.VMEM((2, tokens + 2 * WINDOW, HD), BF16),
+            pltpu.VMEM((tps,) + out_proj.shape, BF16),
+            pltpu.VMEM((tps,) + queries.shape, BF16),
+            pltpu.VMEM((tokens // 2, width), F32),
+            pltpu.VMEM((2 * tokens, width), BF16),
+            pltpu.VMEM((n - 1,) + w_gate.shape, BF16),
+            pltpu.VMEM((n - 1,) + w_up.shape, BF16),
+            pltpu.VMEM((n - 1,) + w_down.shape, BF16),
+            pltpu.VMEM((2 * tokens + 2 * PAD, hidden), F32),
+            pltpu.VMEM((2 * tokens, hidden), F32),
+            pltpu.VMEM((EDGE, hidden), BF16),
+            pltpu.VMEM((EDGE, hidden), BF16),
+            pltpu.VMEM((2 * tokens, hidden), BF16),
+            pltpu.VMEM((tps, 2 * tokens, cols), BF16),
+            pltpu.VMEM((tps, 2 * tokens, cols), BF16),
+            pltpu.VMEM((tokens, cols), BF16),
+            pltpu.VMEM((tokens, cols), BF16),
+            dma((2, 2)), dma((2, 2)),
+            dma((3, 3, groups, CHUNKS)), dma((3, 2, groups, CHUNKS)),
+            cross_sems, cross_sems,
+            dma((3,)), dma((3,)), dma((3,)), dma((3,)), dma((2,)), dma((2,)), dma((1,)), dma((1,)),
+            dma((tps, 2)), dma((tps, 2)), dma((1,)), dma((1,)),
+        ],
+        compiler_params=pltpu.CompilerParams(
+            collective_id=0, has_side_effects=True, vmem_limit_bytes=67043328
+        ),
+    )(queries, keys, values, sink, resid, out_proj, norm_gain[None], w_gate, w_up, conv_w, conv_b[None], w_down)
+
+
+def fits_kernel(sizes, args):
+    groups, n, tps = sizes
+    queries, resid, out_proj, w_gate, w_down = args[0], args[4], args[5], args[7], args[11]
+    part = groups * CHUNKS * EDGE
+    weights = 3 * 2 * n * w_gate.shape[0] * w_gate.shape[1]
+    return (
+        n == 4
+        and tps == 4
+        and groups > 1
+        and w_down.shape[1] == out_proj.shape[1]
+        and w_gate.shape[0] % max(part, 128) == 0
+        and w_down.shape[0] % part == 0
+        and w_down.shape[1] % 256 == 0
+        and w_gate.shape[1] % out_proj.shape[1] == 0
+        and resid.shape[0] % (4 * WINDOW) == 0
+        and weights <= 20 * 2 ** 20
+    )
+
+
+def run_shards(sizes, *args):
+    if fits_kernel(sizes, args):
+        return kernel_shards(sizes, *args)
+    return shards(*args)
+
+
 def solution(mesh):
+    sizes = tuple(mesh.shape[axis] for axis in ("grp", "sp", "tp"))
     return jax.shard_map(
-        shards,
+        functools.partial(run_shards, sizes),
         mesh=mesh,
         in_specs=(
             P(("grp", "sp"), "tp"),

time: 476 us -> 187 us (0.39)
  waiting for transfers between devices: 418 us -> 0 us
  Pallas kernels: 0 us -> 182 us
  matrix products: 29.4 us -> 0 us
  between operations: 13.7 us -> 0.01 us
  starting transfers between devices: 9.21 us -> 0 us
    all_gather x5 -> x0, waiting for transfers between devices: 382 us -> none  [the longest x1 115 us: shards(): lax.all_gather(w_down, 'sp', axis=1, tiled=True)]
    pallas_call x0 -> x1, Pallas kernels: none -> 182 us  [kernel_shards(): pl.pallas_call(functools.partial(layer_kernel, sizes), out_shape=jax.Shap...]
    reduce_scatter x1 -> x0, waiting for transfers between devices: 29.5 us -> none  [shards(): lax.psum_scatter(terms.astype(jnp.bfloat16), 'tp', scatter_dimension=1, t...]
    dot_general x5 -> x0, matrix products: 29.4 us -> none  [the longest x1 15.3 us: shards(): jnp.dot(act, lax.all_gather(w_down, 'sp', axis=1, tiled=True), preferred_...]
    ppermute x4 -> x0, starting transfers between devices: 9.01 us -> none  [the longest x2 6.25 us: with_halo(): lax.ppermute(tail, axis, [(i, (i + 1) % count) for i in range(ends)])]
  transfers between devices with their start and end apart: 10 -> 0, of which waited for: 7 -> 0; matrix products, arithmetic and copies ran while one was open for 3% -> 0% of each run, Pallas kernels for 0% -> 0%
where the time goes in v2:
time: 187 us; the launch traced here: 185 us
  Pallas kernels  182 us (97%)
  local copies, waits for them, and re-layouts  3.16 us (2%)
    pallas_call x1, Pallas kernels, kernel_shards(): pl.pallas_call(functools.partial(layer_kernel, sizes), out_shape=jax.Shap...  182 us

profile of v2, /device:TPU:0, one launch (start us, length us, event | category | flops | bytes accessed | tf_op | source)
XLA Modules:
  0.0 185.0 jit_solution(1555136844349239481)
XLA Ops:
  0.0 1.3 broadcast_in_dim.7.cb_ref
  1.3 181.8 %shard_map.118 = bf16[512,512]{1,0:T(8,128)(2,1)} custom-call(bf16[512,256]{1,0:T(8,128)(2,1)} %q_ref.1, bf16[512,256]{1,0:T(8,128)(2,1)} %k_ref.1, bf16[512,256]{1,0:T(8,128)(2,1)} %v_ref.1, f32[2]{0:T(128)} %sink_ref.1, bf16[512,2048]{1,0:T(8,128)(2,1)} %resid_ref.1, bf16[1024,512]{1,0:T(8,128)(2,1)} %proj_ref.1, f32[1,2048]{1,0:T(1,128)} %bitcast.1, ...), custom_call_target="tpu_custom_call" | custom-call | tf_op jit(solution)/shard_map/pallas_call | solution.py:540
  183.1 1.9 %copy.14 = bf16[512,512]{1,0:T(8,128)(2,1)} copy(bf16[512,512]{1,0:T(8,128)(2,1)} %shard_map.118) | data formatting | bytes 1048576

commit v3 on v2

--- a/solution.py
+++ b/solution.py
@@ -116,10 +116,10 @@
     q_ref, k_ref, v_ref, sink_ref, resid_ref, proj_ref, gain_ref, wg_ref, wu_ref, cw_ref, cb_ref, wd_ref,
     out_ref,
     kv_ext, proj_all, mixed, summed, normed, wg_all, wu_all, wd_all, gate, up, edge, halo, act, terms, parts,
-    ret_out, ret_in,
+    pair_in, ret_out, ret_in,
     halo_send, halo_recv, z_recv, z_send, y_recv, y_send,
     proj_send, proj_recv, mix_send, mix_recv, norm_send, norm_recv, edge_send, edge_recv,
-    term_send, term_recv, ret_send, ret_recv,
+    term_send, term_recv, pair_send, pair_recv, ret_send, ret_recv,
 ):
     groups, n, tps = sizes
     g = lax.axis_index("grp")
@@ -366,14 +366,32 @@
     def edge_copy():
         return remote(edge, halo, edge_send.at[0], edge_recv.at[0], {"sp": s + inward})
 
-    def term_copy(p, own_rows):
-        rows = pl.ds(base if own_rows else other_base, tokens)
-        i = int(own_rows)
+    half_rows = tokens // 2
+    core = lax.rem(t, 2)
+    far_first = (1 - t // 2) * 2
+
+    def is_far(p):
+        return (p // 2) != (t // 2)
+
+    def half_of(i, c):
+        first = (base if i else other_base) + c * half_rows
+        return pl.ds(pl.multiple_of(first, half_rows), half_rows)
+
+    def near_copy(i, u):
+        rows = pl.ds(base if i else other_base, tokens)
+        return remote(terms.at[core_peer, rows], parts.at[u, rows], term_send.at[core_peer, i],
+                      term_recv.at[u, i], {"tp": core_peer})
+
+    def pair_copy(p, i):
+        return remote(terms.at[p, half_of(i, 1 - core)], pair_in.at[lax.rem(p, 2), i],
+                      pair_send.at[lax.rem(p, 2), i], pair_recv.at[lax.rem(p, 2), i], {"tp": core_peer})
+
+    def far_copy(p, i):
+        rows = half_of(i, core)
         return remote(terms.at[p, rows], parts.at[t, rows], term_send.at[p, i], term_recv.at[t, i], {"tp": p})
 
-    def term_arrival(u, own_rows):
-        rows = pl.ds(base if own_rows else other_base, tokens)
-        i = int(own_rows)
+    def far_arrival(c, i):
+        u, rows = far_first + c, half_of(i, c)
         return remote(terms.at[u, rows], parts.at[u, rows], term_send.at[u, i], term_recv.at[u, i], {"tp": u})
 
     tile = 256
@@ -410,31 +428,49 @@
             else:
                 up[:, at] += ub
 
-    def down(slot):
-        if slot is not None:
+    def piece_of(slot):
+        return s + {None: 0, 0: -1, 1: 1, 2: 2}[slot] * inward
+
+    def down(slot, i):
+        if slot is not None and i == 0:
             arrived(2, slot)
-        p = s + {None: 0, 0: -1, 1: 1, 2: 2}[slot] * inward
-        for own_rows in (False, True):
-            rows = pl.ds(base if own_rows else other_base, tokens)
-
-            @pl.loop(0, cols // tile)
-            def _(i):
-                at = pl.ds(pl.multiple_of(i * tile, 128), tile)
-                w = wd_ref[:, at] if slot is None else wd_all[slot, :, at]
-                terms[p, rows, at] = jnp.dot(act[rows, :], w, preferred_element_type=F32).astype(BF16)
-
-            @pl.when(p != t)
-            def _():
-                term_copy(p, own_rows).start()
-
-    def finish(own_rows):
-        rows = pl.ds(base if own_rows else other_base, tokens)
-        out = normed[rows, my_cols].astype(F32) + terms[t, rows, :].astype(F32)
-        for j in range(1, tps):
-            u = lax.rem(t + j, tps)
-            term_arrival(u, own_rows).wait_recv()
-            out = out + parts[u, rows, :].astype(F32)
-        return out.astype(BF16)
+        p = piece_of(slot)
+        rows = pl.ds(base if i else other_base, tokens)
+
+        @pl.loop(0, cols // tile)
+        def _(k):
+            at = pl.ds(pl.multiple_of(k * tile, 128), tile)
+            w = wd_ref[:, at] if slot is None else wd_all[slot, :, at]
+            terms[p, rows, at] = jnp.dot(act[rows, :], w, preferred_element_type=F32).astype(BF16)
+
+        @pl.when(p == core_peer)
+        def _():
+            near_copy(i, t).start()
+
+        @pl.when(is_far(p))
+        def _():
+            pair_copy(p, i).start()
+
+    def settle(slot, i):
+        p = piece_of(slot)
+
+        @pl.when(is_far(p))
+        def _():
+            pair_copy(p, i).wait_recv()
+            rows = half_of(i, core)
+            both = terms[p, rows, :].astype(F32) + pair_in[lax.rem(p, 2), i].astype(F32)
+            terms[p, rows, :] = both.astype(BF16)
+            far_copy(p, i).start()
+
+    def finish(i, ref):
+        near_copy(i, core_peer).wait_recv()
+        for c in range(2):
+            rows = half_of(i, c)
+            out = normed[rows, my_cols].astype(F32) + terms[t, rows, :].astype(F32)
+            out = out + parts[core_peer, rows, :].astype(F32)
+            far_arrival(c, i).wait_recv()
+            out = out + parts[far_first + c, rows, :].astype(F32)
+            ref[pl.ds(c * half_rows, half_rows), :] = out.astype(BF16)
 
     @pl.when(outer)
     def _():
@@ -489,20 +525,24 @@
             silu = conv / (1.0 + jnp.exp(-conv))
             act[:, at] = (silu * up[:, at].astype(BF16).astype(F32)).astype(BF16)
 
-        down(None)
-        down(1)
-        down(2)
-        down(0)
-        ret_out[...] = finish(False)
+        steps = [(slot, i) for i in range(2) for slot in (None, 1, 2, 0)]
+        for at, (slot, i) in enumerate(steps):
+            down(slot, i)
+            if at:
+                settle(*steps[at - 1])
+        settle(*steps[-1])
+        finish(0, ret_out)
         ret_copy().start()
-        out_ref[...] = finish(True)
+        finish(1, out_ref)
 
         ret_copy().wait_send()
         edge_copy().wait_send()
         norm_over(False).wait_send()
-        for j in range(1, tps):
-            for own_rows in (False, True):
-                term_copy(lax.rem(t + j, tps), own_rows).wait_send()
+        for i in range(2):
+            near_copy(i, t).wait_send()
+            for c in range(2):
+                pair_copy(far_first + c, i).wait_send()
+                far_copy(far_first + c, i).wait_send()
         for m, c in pieces:
             hop(m, None, 1, 0, c).wait_send()
             hop(m, 0, 2, 0, c).wait_send()
@@ -558,13 +598,14 @@
             pltpu.VMEM((2 * tokens, hidden), BF16),
             pltpu.VMEM((tps, 2 * tokens, cols), BF16),
             pltpu.VMEM((tps, 2 * tokens, cols), BF16),
+            pltpu.VMEM((2, 2, tokens // 2, cols), BF16),
             pltpu.VMEM((tokens, cols), BF16),
             pltpu.VMEM((tokens, cols), BF16),
             dma((2, 2)), dma((2, 2)),
             dma((3, 3, groups, CHUNKS)), dma((3, 2, groups, CHUNKS)),
             cross_sems, cross_sems,
             dma((3,)), dma((3,)), dma((3,)), dma((3,)), dma((2,)), dma((2,)), dma((1,)), dma((1,)),
-            dma((tps, 2)), dma((tps, 2)), dma((1,)), dma((1,)),
+            dma((tps, 2)), dma((tps, 2)), dma((2, 2)), dma((2, 2)), dma((1,)), dma((1,)),
         ],
         compiler_params=pltpu.CompilerParams(
             collective_id=0, has_side_effects=True, vmem_limit_bytes=67043328

time: 187 us -> 166 us (0.89)
  Pallas kernels: 182 us -> 161 us
    pallas_call x1, Pallas kernels: 182 us -> 161 us  [kernel_shards(): pl.pallas_call(functools.partial(layer_kernel, sizes), out_shape=jax.Shap...]
where the time goes in v3:
time: 166 us; the launch traced here: 164 us
  Pallas kernels  161 us (97%)
  local copies, waits for them, and re-layouts  3.16 us (2%)
    pallas_call x1, Pallas kernels, kernel_shards(): pl.pallas_call(functools.partial(layer_kernel, sizes), out_shape=jax.Shap...  161 us

profile of v3, /device:TPU:0, one launch (start us, length us, event | category | flops | bytes accessed | tf_op | source)
XLA Modules:
  0.0 163.8 jit_solution(9201068196071967656)
XLA Ops:
  0.0 1.3 broadcast_in_dim.7.cb_ref
  1.3 160.7 %shard_map.118 = bf16[512,512]{1,0:T(8,128)(2,1)} custom-call(bf16[512,256]{1,0:T(8,128)(2,1)} %q_ref.1, bf16[512,256]{1,0:T(8,128)(2,1)} %k_ref.1, bf16[512,256]{1,0:T(8,128)(2,1)} %v_ref.1, f32[2]{0:T(128)} %sink_ref.1, bf16[512,2048]{1,0:T(8,128)(2,1)} %resid_ref.1, bf16[1024,512]{1,0:T(8,128)(2,1)} %proj_ref.1, f32[1,2048]{1,0:T(1,128)} %bitcast.1, ...), custom_call_target="tpu_custom_call" | custom-call | tf_op jit(solution)/shard_map/pallas_call | solution.py:580
  162.0 1.9 %copy.14 = bf16[512,512]{1,0:T(8,128)(2,1)} copy(bf16[512,512]{1,0:T(8,128)(2,1)} %shard_map.118) | data formatting | bytes 1048576

commit v4 on v3

--- a/solution.py
+++ b/solution.py
@@ -235,7 +235,7 @@
 
     @pl.when(inner)
     def _():
-        for m, c in pieces:
+        for m, c in pieces[:2 * CHUNKS]:
             hop(m, None, 1, 0, c).start()
 
     for step in (1, 0):
@@ -488,17 +488,19 @@
     @pl.when(inner)
     def _():
         relay_near(1)
-        relay_near(2)
+        for m, c in pieces[2 * CHUNKS:]:
+            hop(m, None, 1, 0, c).start()
         relay_far(0)
+        relay_far(1)
         norm_in_arrival().wait_recv()
         norm_over(False).start()
-        relay_far(1)
+        relay_near(2)
         norm_over(True).wait_recv()
         gate_up(None)
         gate_up(1)
+        gate_up(2)
         relay_far(2)
         gate_up(0)
-        gate_up(2)
 
         at_edge = pl.multiple_of(PAD + (1 - s // (n // 2)) * (rows2 - EDGE), PAD)
         edge[...] = gate[pl.ds(at_edge, EDGE), :].astype(BF16)
@@ -525,7 +527,7 @@
             silu = conv / (1.0 + jnp.exp(-conv))
             act[:, at] = (silu * up[:, at].astype(BF16).astype(F32)).astype(BF16)
 
-        steps = [(slot, i) for i in range(2) for slot in (None, 1, 2, 0)]
+        steps = [(slot, i) for slots in ((None, 1), (0, 2)) for i in range(2) for slot in slots]
         for at, (slot, i) in enumerate(steps):
             down(slot, i)
             if at:

time: 166 us -> 165 us (level); the launches traced: 164 us -> 165 us
  no operation moved by 1% of the time
where the time goes in v4:
time: 165 us
  Pallas kernels  162 us (98%)
  local copies, waits for them, and re-layouts  3.16 us (2%)
    pallas_call x1, Pallas kernels, kernel_shards(): pl.pallas_call(functools.partial(layer_kernel, sizes), out_shape=jax.Shap...  162 us

profile of v4, /device:TPU:0, one launch (start us, length us, event | category | flops | bytes accessed | tf_op | source)
XLA Modules:
  0.0 165.2 jit_solution(1850099578884726359)
XLA Ops:
  0.0 1.3 broadcast_in_dim.7.cb_ref
  1.3 162.0 %shard_map.118 = bf16[512,512]{1,0:T(8,128)(2,1)} custom-call(bf16[512,256]{1,0:T(8,128)(2,1)} %q_ref.1, bf16[512,256]{1,0:T(8,128)(2,1)} %k_ref.1, bf16[512,256]{1,0:T(8,128)(2,1)} %v_ref.1, f32[2]{0:T(128)} %sink_ref.1, bf16[512,2048]{1,0:T(8,128)(2,1)} %resid_ref.1, bf16[1024,512]{1,0:T(8,128)(2,1)} %proj_ref.1, f32[1,2048]{1,0:T(1,128)} %bitcast.1, ...), custom_call_target="tpu_custom_call" | custom-call | tf_op jit(solution)/shard_map/pallas_call | solution.py:582
  163.3 1.9 %copy.14 = bf16[512,512]{1,0:T(8,128)(2,1)} copy(bf16[512,512]{1,0:T(8,128)(2,1)} %shard_map.118) | data formatting | bytes 1048576
